TPU v7x, 32 devices: a whole 2x2x4 slice. The times are simulated.
32 devices in a mesh: ep: 4 (over y, x), tp: 8 (over z, core).
Axes of the slice: x: 2, y: 2, z: 4, core: 2. Of those that a mesh axis runs over, the one named last changes fastest.
Arguments:
- tokens: bfloat16 [64, 2048], P('ep'), may hold values from -6 to 6
- routes: int32 [64, 4], P('ep'), may hold values from 0 to 7, all different within a row; in each aligned block of 16 rows (0 to 15, 16 to 31, ...) at most 16 rows name the same one
- route_weight: float32 [64, 4], P('ep'), may hold values from 0.2 to 1
- mixer_gain: float32 [2048], replicated, may hold values from 0.1 to 1.9
- gate_weight: bfloat16 [2048, 4096], P(None, 'tp'), may hold values from -0.125 to 0.125
- input_weight: bfloat16 [2048, 4096], P(None, 'tp'), may hold values from -0.125 to 0.125
- step_weight: bfloat16 [2048, 64], P(None, 'tp'), may hold values from -0.125 to 0.125
- write_weight: bfloat16 [2048, 512], P('tp'), may hold values from -0.125 to 0.125
- read_weight: bfloat16 [2048, 512], P('tp'), may hold values from -0.125 to 0.125
- step_bias: float32 [64], P('tp'), may hold values from -3 to 0.5
- decay_log: float32 [64], P('tp'), may hold values from -2 to 0.5
- decay_jolt: float32 [64, 64], P('ep', 'tp'), may hold values from -1 to 0
- filter_taps: bfloat16 [4, 4096], P(None, 'tp'), may hold values from -3 to 3
- filter_state: bfloat16 [64, 3, 4096], P('ep', None, 'tp'), may hold values from -6 to 6
- scan_state: float32 [64, 64, 64, 128], P('ep', 'tp'), may hold values from -2 to 2
- skip_gain: float32 [64], P('tp'), may hold values from 0.5 to 2
- head_gain: float32 [4096], P('tp'), may hold values from 0.1 to 1.9
- output_weight: bfloat16 [4096, 2048], P('tp'), may hold values from -0.09375 to 0.09375
- channel_gain: float32 [2048], replicated, may hold values from 0.1 to 1.9
- expert_gate: bfloat16 [8, 2048, 2048], P('ep', None, 'tp'), may hold values from -0.125 to 0.125
- expert_up: bfloat16 [8, 2048, 2048], P('ep', None, 'tp'), may hold values from -0.125 to 0.125
- expert_down: bfloat16 [8, 2048, 2048], P('ep', 'tp'), may hold values from -0.125 to 0.125
- shared_gate: bfloat16 [2048, 2048], P(None, 'tp'), may hold values from -0.125 to 0.125
- shared_up: bfloat16 [2048, 2048], P(None, 'tp'), may hold values from -0.125 to 0.125
- shared_down: bfloat16 [2048, 2048], P('tp'), may hold values from -0.125 to 0.125
Outputs:
- layer_out: bfloat16 [64, 2048], P('ep', 'tp')
- new_state: float32 [64, 64, 64, 128], P('ep', 'tp')
- new_filter: bfloat16 [64, 3, 4096], P('ep', None, 'tp')
Inputs may be any that keep to these rules, and one draw needn't show every extreme that they name: `routes`: each row names 4 different experts. In each aligned block of 16 rows (the rows of one index of ep) no expert is named by more than 16 rows, a bound that some block reaches.
All inputs are finite; a program needn't handle non-finite values.
Results may differ from a plain program's by a relative error of at most 0.025.
Values may be sent and summed in bfloat16 or wider, within the bound.
A program may use at most 64 MiB of HBM per device.

v0:
```python
import jax
import jax.numpy as jnp
from jax import lax
from jax.sharding import PartitionSpec as P

HEADS = 64
HEAD_DIM = 64
GROUPS = 4
STATE = 128
EPS = 1e-06


def rms_normed(values, scaling):
    mean_square = jnp.mean(values * values, axis=-1, keepdims=True)
    return values * lax.rsqrt(mean_square + EPS) * scaling


def route_targets(route_ids, experts, capacity):
    count_rows, top_picks = route_ids.shape
    flattened = route_ids.reshape(count_rows * top_picks)
    onehot = (flattened[:, None] == jnp.arange(experts, dtype=jnp.int32)[None, :]).astype(jnp.int32)
    before = jnp.cumsum(onehot, axis=0) - onehot
    slot_index = jnp.sum(before * onehot, axis=1)
    return (flattened * capacity + slot_index).reshape(count_rows, top_picks)


def expert_terms(token_rows, expert_gate, expert_up, expert_down):
    gate_part = jnp.einsum(
        "ajcd,jdf->ajcf", token_rows, expert_gate, preferred_element_type=jnp.float32
    )
    up_part = jnp.einsum(
        "ajcd,jdf->ajcf", token_rows, expert_up, preferred_element_type=jnp.float32
    )
    hidden = (jax.nn.silu(gate_part) * up_part).astype(jnp.bfloat16)
    return jnp.einsum("ajcf,jfd->ajcd", hidden, expert_down, preferred_element_type=jnp.float32)


def on_device(
    tokens,
    routes,
    route_weight,
    mixer_gain,
    gate_weight,
    input_weight,
    step_weight,
    write_weight,
    read_weight,
    step_bias,
    decay_log,
    decay_jolt,
    filter_taps,
    filter_state,
    scan_state,
    skip_gain,
    head_gain,
    output_weight,
    channel_gain,
    expert_gate,
    expert_up,
    expert_down,
    shared_gate,
    shared_up,
    shared_down,
):
    seq_rows, model_width = tokens.shape
    tp_count = lax.axis_size("tp")
    tp_index = lax.axis_index("tp")
    ep_count = lax.axis_size("ep")
    col_count = model_width // tp_count
    col_start = tp_index * col_count
    tokens_f = tokens.astype(jnp.float32)
    normed = rms_normed(tokens_f, mixer_gain).astype(jnp.bfloat16)
    feature_rows = write_weight.shape[0]
    own_features = lax.dynamic_slice_in_dim(normed, tp_index * feature_rows, feature_rows, 1)
    write_part = jnp.dot(own_features, write_weight, preferred_element_type=jnp.float32)
    read_part = jnp.dot(own_features, read_weight, preferred_element_type=jnp.float32)
    write_in, read_in = (
        lax.psum(write_part.astype(jnp.bfloat16), "tp").astype(jnp.float32),
        lax.psum(read_part.astype(jnp.bfloat16), "tp").astype(jnp.float32),
    )
    gate_rows = jnp.dot(normed, gate_weight, preferred_element_type=jnp.float32).astype(
        jnp.bfloat16
    )
    input_rows = jnp.dot(normed, input_weight, preferred_element_type=jnp.float32).astype(
        jnp.bfloat16
    )
    step_raw = jnp.dot(normed, step_weight, preferred_element_type=jnp.float32)
    window = jnp.concatenate([filter_state, input_rows[:, None, :]], axis=1)
    filtered = jax.nn.silu(
        jnp.sum(window.astype(jnp.float32) * filter_taps.astype(jnp.float32)[None], axis=1)
    )
    step_size = jax.nn.softplus(step_raw + step_bias)
    log_decay = decay_jolt - jnp.exp(decay_log) * step_size
    heads_here = step_bias.shape[0]
    head_input = filtered.reshape(seq_rows, heads_here, HEAD_DIM)
    group_index = tp_index * heads_here // (HEADS // GROUPS)
    write_vec = jax.nn.silu(lax.dynamic_slice_in_dim(write_in, group_index * STATE, STATE, 1))
    read_vec = jax.nn.silu(lax.dynamic_slice_in_dim(read_in, group_index * STATE, STATE, 1))
    new_state = (
        jnp.exp(log_decay)[:, :, None, None] * scan_state
        + (step_size[:, :, None] * head_input)[:, :, :, None] * write_vec[:, None, None, :]
    )
    readout = jnp.einsum("shpn,sn->shp", new_state, read_vec, precision=lax.Precision.HIGHEST)
    readout = readout + skip_gain[None, :, None] * head_input
    gate_heads = gate_rows.astype(jnp.float32).reshape(seq_rows, heads_here, HEAD_DIM)
    gated = rms_normed(readout * jax.nn.silu(gate_heads), head_gain.reshape(heads_here, HEAD_DIM))
    gated = gated.astype(jnp.bfloat16).reshape(seq_rows, heads_here * HEAD_DIM)
    mixer_part = jnp.dot(gated, output_weight, preferred_element_type=jnp.float32)
    mixed = lax.psum(mixer_part.astype(jnp.bfloat16), "tp")
    resid = (tokens_f + mixed.astype(jnp.float32)).astype(jnp.bfloat16)
    normed_ffn = rms_normed(resid.astype(jnp.float32), channel_gain).astype(jnp.bfloat16)
    resid_own = lax.dynamic_slice_in_dim(resid, col_start, col_count, 1)
    shared_hidden = (
        jax.nn.silu(jnp.dot(normed_ffn, shared_gate, preferred_element_type=jnp.float32))
        * jnp.dot(normed_ffn, shared_up, preferred_element_type=jnp.float32)
    ).astype(jnp.bfloat16)
    shared_part = jnp.dot(shared_hidden, shared_down, preferred_element_type=jnp.float32)
    local_experts = expert_gate.shape[0]
    experts = local_experts * ep_count
    top_picks = routes.shape[1]
    capacity = 2 * seq_rows * top_picks // experts
    targets = route_targets(routes, experts, capacity)
    slot_ids = jnp.arange(experts * capacity, dtype=jnp.int32)
    dispatch = jnp.sum((targets[None, :, :] == slot_ids[:, None, None]).astype(jnp.float32), axis=2)
    send_rows = jnp.dot(
        dispatch.astype(jnp.bfloat16), normed_ffn, preferred_element_type=jnp.float32
    )
    send_rows = send_rows.astype(jnp.bfloat16).reshape(
        ep_count, local_experts, capacity, model_width
    )
    terms = expert_terms(
        lax.all_to_all(send_rows, "ep", split_axis=0, concat_axis=0, tiled=True),
        expert_gate,
        expert_up,
        expert_down,
    )
    routed_parts, shared_sum = (
        lax.psum_scatter(terms.astype(jnp.bfloat16), "tp", scatter_dimension=3, tiled=True).astype(
            jnp.float32
        ),
        lax.psum_scatter(
            shared_part.reshape(1, 1, seq_rows, model_width).astype(jnp.bfloat16),
            "tp",
            scatter_dimension=3,
            tiled=True,
        ).astype(jnp.float32),
    )
    expert_rows = routed_parts.astype(jnp.bfloat16)
    returned = lax.all_to_all(expert_rows, "ep", split_axis=0, concat_axis=0, tiled=True)
    returned = returned.reshape(experts * capacity, col_count).astype(jnp.float32)
    combine = jnp.sum(
        jnp.where(targets[:, :, None] == slot_ids[None, None, :], route_weight[:, :, None], 0.0),
        axis=1,
    )
    routed_sum = jnp.dot(combine, returned, precision=lax.Precision.HIGHEST)
    layer_out = (resid_own.astype(jnp.float32) + shared_sum[0, 0] + routed_sum).astype(jnp.bfloat16)
    return (layer_out, new_state, window[:, 1:, :])


def solution(mesh):
    in_specs = (
        P("ep", None),
        P("ep", None),
        P("ep", None),
        P(),
        P(None, "tp"),
        P(None, "tp"),
        P(None, "tp"),
        P("tp", None),
        P("tp", None),
        P("tp"),
        P("tp"),
        P("ep", "tp"),
        P(None, "tp"),
        P("ep", None, "tp"),
        P("ep", "tp", None, None),
        P("tp"),
        P("tp"),
        P("tp", None),
        P(),
        P("ep", None, "tp"),
        P("ep", None, "tp"),
        P("ep", "tp", None),
        P(None, "tp"),
        P(None, "tp"),
        P("tp", None),
    )
    out_specs = (P("ep", "tp"), P("ep", "tp", None, None), P("ep", None, "tp"))
    return jax.shard_map(
        on_device, mesh=mesh, in_specs=in_specs, out_specs=out_specs, check_vma=False
    )
```

profile of v0, /device:TPU:0, one launch (start us, length us, event | category | flops | bytes accessed | tf_op | source)
XLA Modules:
  0.0 199.6 jit_solution(1012858224445261043)
XLA Ops:
  7.3 1.1 fusion.31
  8.4 0.9 fusion.33
  9.4 2.0 fusion.21
  11.4 0.1 reshape.93
  11.5 0.1 convolution_convert_fusion.6
  11.6 0.2 convolution_convert_fusion.5
  11.8 0.1 subtract_exponential_fusion
  12.0 2.0 fusion.22
  14.3 30.3 %all-reduce = (bf16[16,512]{1,0:T(8,128)(2,1)S(1)}, bf16[16,512]{1,0:T(8,128)(2,1)S(1)}) all-reduce(bf16[16,512]{1,0:T(8,128)(2,1)S(1)} %convolution_convert_fusion.6, bf16[16,512]{1,0:T(8,128)(2,1)S(1)} %convolution_convert_fusion.5), channel_id=1, replica_groups=mesh['ep'=4,'tp'=8] {'tp'}, use_global_device_ids=true, to_apply=%region_2.0 | all-reduce | flops 16384 | bytes 65536 | tf_op jit(solution)/shard_map/psum | solution.py:78
  44.7 3.1 %multiply_add_fusion = f32[16,8,64,128]{3,2,1,0:T(8,128)S(1)} fusion(f32[16,8,64,128]{3,2,1,0:T(8,128)} %param.39, f32[16,128]{1,0:T(8,128)S(1)} %get-tuple-element.12, f32[16,8,64]{2,1,0:T(8,128)S(1)} %broadcast_multiply_fusion, f32[16,8]{1,0:T(8,128)S(1)} %copy.58), kind=kLoop, calls=%fused_computation | loop fusion | flops 3145728 | bytes 8430080 | tf_op jit(solution)/shard_map/add | solution.py:100
  47.8 9.8 %fusion.68 = f32[16,1,8,64]{3,1,2,0:T(1,128)S(1)} fusion(f32[16,8,64,128]{3,2,1,0:T(8,128)S(1)} %multiply_add_fusion, f32[16,128,1,1]{1,2,3,0:T(1,128)S(1)} %bitcast.72), kind=kOutput, calls=%fused_computation.95 | convolution fusion | flops 12582912 | bytes 4235264 | tf_op jit(solution)/shard_map/shpn,sn->shp/dot_general | solution.py:103
  57.7 0.2 multiply_reduce_fusion.1
  58.0 0.1 reshape.89
  58.1 2.6 %convolution_convert_fusion.3 = bf16[16,2048]{1,0:T(8,128)(2,1)} fusion(bf16[16,512]{1,0:T(8,128)(2,1)S(1)} %reshape.89, bf16[512,2048]{1,0:T(8,128)(2,1)} %param.42), kind=kOutput, calls=%fused_computation.5 | convolution fusion | flops 33587200 | bytes 2179072 | tf_op jit(solution)/shard_map/dot_general | solution.py:108
  60.8 0.1 eq.20
  61.0 0.1 reduce_window_sum.11
  61.1 0.2 select_reduce_fusion.1
  61.4 0.1 copy.61
  61.5 52.3 %all-reduce.3.cloned.1.call-done = bf16[16,2048]{1,0:T(8,128)(2,1)} async-done(((bf16[16,2048]{1,0:T(8,128)(2,1)}), bf16[16,2048]{1,0:T(8,128)(2,1)}) %all-reduce.3.cloned.1.call-update) | async-done | bytes 65552 | tf_op jit(solution)/shard_map/psum | solution.py:109
  113.9 1.0 fusion.28
  114.9 0.3 convolution_convert_fusion.1
  115.2 10.6 %all_to_all.10 = bf16[4,2,16,2048]{3,2,1,0:T(8,128)(2,1)S(1)} all-to-all(bf16[4,2,16,2048]{3,2,1,0:T(8,128)(2,1)S(1)} %bitcast.69), channel_id=1, replica_groups=mesh['ep'=4,'tp'=8] {'ep'}, dimensions={0} | all-to-all | bytes 1048576 | tf_op jit(solution)/shard_map/all_to_all | solution.py:132
  125.8 2.1 %fusion.7 = f32[4,2,16,256]{3,2,0,1:T(8,128)S(1)} fusion(bf16[2,2048,256]{2,1,0:T(8,128)(2,1)} %param.44, bf16[4,2,16,2048]{3,2,1,0:T(8,128)(2,1)S(1)} %all_to_all.10), kind=kOutput, calls=%fused_computation.12 | convolution fusion | flops 134217728 | bytes 2752512 | tf_op jit(solution)/shard_map/ajcd,jdf->ajcf/dot_general | solution.py:28
  127.8 3.3 %fusion = bf16[4,2,16,2048]{3,2,0,1:T(8,128)(2,1)} fusion(bf16[2,256,2048]{2,1,0:T(8,128)(2,1)S(1)} %copy-done, bf16[2,2048,256]{2,1,0:T(8,128)(2,1)} %param.45, bf16[4,2,16,2048]{3,2,1,0:T(8,128)(2,1)S(1)} %all_to_all.10, f32[4,2,16,256]{3,2,0,1:T(8,128)S(1)} %fusion.7), kind=kOutput, calls=%fused_computation.3 | convolution fusion | flops 268894208 | bytes 5373952 | tf_op jit(solution)/shard_map/ajcf,jfd->ajcd/dot_general | solution.py:35
  131.2 1.5 fusion.65
  132.7 2.9 %fusion.1 = bf16[1,1,16,2048]{3,2,1,0:T(8,128)(2,1)} fusion(bf16[256,2048]{1,0:T(8,128)(2,1)} %param.49, bf16[2048,256]{1,0:T(8,128)(2,1)} %param.48, f32[16,256]{1,0:T(8,128)S(1)} %fusion.65, bf16[16,2048]{1,0:T(8,128)(2,1)S(1)} %get-tuple-element.6, f32[2048]{0:T(1024)S(1)} %copy-done.6, f32[16]{0:T(128)S(1)} %add_rsqrt_fusion.1), kind=kOutput, calls=%fused_computation.6 | convolution fusion | flops 33742848 | bytes 2252864 | tf_op jit(solution)/shard_map/dot_general | solution.py:117
  135.8 25.0 %reduce-scatter.5.cloned.1.call-done = bf16[4,2,16,256]{3,2,0,1:T(8,128)(2,1)} async-done(((bf16[4,2,16,2048]{3,2,0,1:T(8,128)(2,1)}), bf16[4,2,16,256]{3,2,0,1:T(8,128)(2,1)}) %reduce-scatter.5.cloned.1.call-update) | async-done | bytes 65552 | tf_op jit(solution)/shard_map/reduce_scatter | solution.py:138
  160.8 1.5 copy.64
  162.2 3.6 %all-to-all-start.1 = ((bf16[4,2,16,256]{3,2,1,0:T(8,128)(2,1)}), bf16[4,2,16,256]{3,2,1,0:T(8,128)(2,1)S(1)}, u32[]{:S(2)}, u32[]{:S(2)}) async-start(bf16[4,2,16,256]{3,2,1,0:T(8,128)(2,1)} %copy.64), calls=%async_computation.3 | async-start | bytes 131072 | tf_op jit(solution)/shard_map/all_to_all | solution.py:149
  165.9 0.6 fusion.41
  166.5 25.2 %reduce-scatter.3.cloned.1.call-done = bf16[1,1,16,256]{3,2,1,0:T(8,128)(2,1)} async-done(((bf16[1,1,16,2048]{3,2,1,0:T(8,128)(2,1)}), bf16[1,1,16,256]{3,2,1,0:T(8,128)(2,1)}) %reduce-scatter.3.cloned.1.call-update) | async-done | bytes 8208 | tf_op jit(solution)/shard_map/reduce_scatter | solution.py:141
  191.7 1.4 fusion.24
  (58 shorter events, 1.2 us)
Async XLA Ops:
  7.2 120.7 %copy-start = (bf16[2,256,2048]{2,1,0:T(8,128)(2,1)S(1)}, bf16[2,256,2048]{2,1,0:T(8,128)(2,1)}, u32[]{:S(2)}) copy-start(bf16[2,256,2048]{2,1,0:T(8,128)(2,1)} %param.46) | copy-start | bytes 6291460
  7.2 4.3 %copy-start.3 = (bf16[256,512]{1,0:T(8,128)(2,1)S(1)}, bf16[256,512]{1,0:T(8,128)(2,1)}, u32[]{:S(2)}) copy-start(bf16[256,512]{1,0:T(8,128)(2,1)} %param.32) | copy-start | bytes 786436
  7.2 4.4 %copy-start.4 = (bf16[256,512]{1,0:T(8,128)(2,1)S(1)}, bf16[256,512]{1,0:T(8,128)(2,1)}, u32[]{:S(2)}) copy-start(bf16[256,512]{1,0:T(8,128)(2,1)} %param.33) | copy-start | bytes 786436
  7.2 4.6 %copy-start.14 = (f32[8]{0:T(128)S(1)}, f32[8]{0:T(128)}, u32[]{:S(2)}) copy-start(f32[8]{0:T(128)} %param.35) | copy-start | bytes 100
  7.2 4.6 %copy-start.13 = (f32[16,8]{0,1:T(8,128)S(1)}, f32[16,8]{0,1:T(8,128)}, u32[]{:S(2)}) copy-start(f32[16,8]{0,1:T(8,128)} %param.36) | copy-start | bytes 1540
  7.2 4.6 %copy-start.15 = (f32[8]{0:T(128)S(1)}, f32[8]{0:T(128)}, u32[]{:S(2)}) copy-start(f32[8]{0:T(128)} %param.34) | copy-start | bytes 100
  7.2 4.6 %copy-start.12 = (bf16[2048,8]{0,1:T(8,128)(2,1)S(1)}, bf16[2048,8]{0,1:T(8,128)(2,1)}, u32[]{:S(2)}) copy-start(bf16[2048,8]{0,1:T(8,128)(2,1)} %param.31) | copy-start | bytes 98308
  7.2 106.6 %all-reduce.3.cloned.1.call-start = ((), (), s32[]{:S(2)}) async-start(), calls=%async_computation.4 | async-start | bytes 131072 | tf_op jit(solution)/shard_map/psum | solution.py:109
  9.4 4.6 %copy-start.8 = (bf16[4,512]{1,0:T(4,128)(2,1)S(1)}, bf16[4,512]{1,0:T(4,128)(2,1)}, u32[]{:S(2)}) copy-start(bf16[4,512]{1,0:T(4,128)(2,1)} %param.37) | copy-start | bytes 12292
  9.4 4.7 %copy-start.5 = (bf16[16,3,512]{2,0,1:T(8,128)(2,1)S(1)}, bf16[16,3,512]{2,0,1:T(8,128)(2,1)}, u32[]{:S(2)}) copy-start(bf16[16,3,512]{2,0,1:T(8,128)(2,1)} %param.38) | copy-start | bytes 147460
  11.4 2.8 %copy-start.9 = (f32[512]{0:T(512)S(1)}, f32[512]{0:T(512)}, u32[]{:S(2)}) copy-start(f32[512]{0:T(512)} %param.41) | copy-start | bytes 6148
  47.8 9.8 %copy-start.1 = (f32[16,8,64,128]{3,2,1,0:T(8,128)}, f32[16,8,64,128]{3,2,1,0:T(8,128)S(1)}, u32[]{:S(2)}) copy-start(f32[16,8,64,128]{3,2,1,0:T(8,128)S(1)} %multiply_add_fusion) | copy-start | bytes 12582916
  47.8 9.9 %copy-start.11 = (f32[8]{0:T(128)S(1)}, f32[8]{0:T(128)}, u32[]{:S(2)}) copy-start(f32[8]{0:T(128)} %param.40) | copy-start | bytes 100
  57.6 3.1 %copy-start.7 = (s32[16,4]{0,1:T(4,128)S(1)}, s32[16,4]{0,1:T(4,128)}, u32[]{:S(2)}) copy-start(s32[16,4]{0,1:T(4,128)} %param.26) | copy-start | bytes 772
  57.6 56.2 %copy-start.2 = (bf16[16,2048]{1,0:T(8,128)(2,1)S(1)}, bf16[16,2048]{1,0:T(8,128)(2,1)}, u32[]{:S(2)}) copy-start(bf16[16,2048]{1,0:T(8,128)(2,1)} %param.25) | copy-start | bytes 196612
  57.7 57.2 %copy-start.6 = (f32[2048]{0:T(1024)S(1)}, f32[2048]{0:T(1024)}, u32[]{:S(2)}) copy-start(f32[2048]{0:T(1024)} %param.43) | copy-start | bytes 24580
  60.7 100.1 %reduce-scatter.5.cloned.1.call-start = ((), (), s32[]{:S(2)}) async-start(), calls=%async_computation.6 | async-start | bytes 589824 | tf_op jit(solution)/shard_map/reduce_scatter | solution.py:138
  131.1 4.6 %copy-start.10 = (f32[16,4]{0,1:T(4,128)S(1)}, f32[16,4]{0,1:T(4,128)}, u32[]{:S(2)}) copy-start(f32[16,4]{0,1:T(4,128)} %param.27) | copy-start | bytes 772
  131.1 60.5 %reduce-scatter.3.cloned.1.call-start = ((), (), s32[]{:S(2)}) async-start(), calls=%async_computation.5 | async-start | bytes 73728 | tf_op jit(solution)/shard_map/reduce_scatter | solution.py:141
  162.2 29.4 %all-to-all-start.1 = ((bf16[4,2,16,256]{3,2,1,0:T(8,128)(2,1)}), bf16[4,2,16,256]{3,2,1,0:T(8,128)(2,1)S(1)}, u32[]{:S(2)}, u32[]{:S(2)}) async-start(bf16[4,2,16,256]{3,2,1,0:T(8,128)(2,1)} %copy.64), calls=%async_computation.3 | async-start | bytes 131072 | tf_op jit(solution)/shard_map/all_to_all | solution.py:149
Sparse Core Ops, SparseCore 0:
  60.8 53.0 all-reduce.2
  131.3 29.4 reduce-scatter.4
  163.0 28.6 reduce-scatter.2
where the time goes:
time: 200 us
  waiting for transfers between devices  103 us (52%)
  blocking collectives  40.9 us (20%)
  matrix products  28.4 us (14%)
  between operations  14 us (7%)
  other arithmetic  7.67 us (4%)
  starting transfers between devices  3.77 us (2%)
  local copies, waits for them, and re-layouts  2.39 us (1%)
    psum x1, waiting for transfers between devices, on_device(): mixed = lax.psum(mixer_part.astype(jnp.bfloat16), 'tp')  52.3 us
    psum x1, blocking collectives, on_device(): lax.psum(write_part.astype(jnp.bfloat16), 'tp').astype(jnp.float32)  30.3 us
    reduce_scatter x1, waiting for transfers between devices, on_device(): lax.psum_scatter(shared_part.reshape(1, 1, seq_rows, model_width).astype(...  25.2 us
    reduce_scatter x1, waiting for transfers between devices, on_device(): lax.psum_scatter(terms.astype(jnp.bfloat16), 'tp', scatter_dimension=3, t...  25 us
    all_to_all x1, blocking collectives, on_device(): lax.all_to_all(send_rows, 'ep', split_axis=0, concat_axis=0, tiled=True)  10.6 us
    dot_general x1, matrix products, on_device(): jnp.einsum('shpn,sn->shp', new_state, read_vec, precision=lax.Precision.H...  9.81 us
  transfers between devices with their start and end apart: 4, of which 3 were waited for; matrix products, arithmetic and copies ran while one was open for 4% of the time, Pallas kernels for 0%

commit v1 on v0

--- a/solution.py
+++ b/solution.py
@@ -75,7 +75,7 @@
     write_part = jnp.dot(own_features, write_weight, preferred_element_type=jnp.float32)
     read_part = jnp.dot(own_features, read_weight, preferred_element_type=jnp.float32)
     write_in, read_in = (
-        lax.psum(write_part.astype(jnp.bfloat16), "tp").astype(jnp.float32),
+        jnp.sum(lax.all_gather(write_part.astype(jnp.bfloat16), "tp"), axis=0).astype(jnp.float32),
         lax.psum(read_part.astype(jnp.bfloat16), "tp").astype(jnp.float32),
     )
     gate_rows = jnp.dot(normed, gate_weight, preferred_element_type=jnp.float32).astype(

time: 200 us -> 215 us (1.075)
  blocking collectives: 40.9 us -> 55.4 us
    all_gather x0 -> x1, blocking collectives: none -> 15.7 us  [on_device(): lax.all_gather(write_part.astype(jnp.bfloat16), 'tp')]
  transfers between devices with their start and end apart: 4 -> 4, of which waited for: 3 -> 3; matrix products, arithmetic and copies ran while one was open for 4% -> 3% of each run, Pallas kernels for 0% -> 0%
where the time goes in v1:
time: 215 us; the launch traced here: 214 us
  waiting for transfers between devices  103 us (48%)
  blocking collectives  55.4 us (26%)
  matrix products  28.4 us (13%)
  between operations  14.1 us (7%)
  other arithmetic  7.7 us (4%)
  starting transfers between devices  3.63 us (2%)
  local copies, waits for them, and re-layouts  2.39 us (1%)
    psum x1, waiting for transfers between devices, on_device(): mixed = lax.psum(mixer_part.astype(jnp.bfloat16), 'tp')  52.3 us
    psum x1, blocking collectives, on_device(): lax.psum(read_part.astype(jnp.bfloat16), 'tp').astype(jnp.float32)  29 us
    reduce_scatter x1, waiting for transfers between devices, on_device(): lax.psum_scatter(shared_part.reshape(1, 1, seq_rows, model_width).astype(...  25.2 us
    reduce_scatter x1, waiting for transfers between devices, on_device(): lax.psum_scatter(terms.astype(jnp.bfloat16), 'tp', scatter_dimension=3, t...  25.1 us
    all_gather x1, blocking collectives, on_device(): lax.all_gather(write_part.astype(jnp.bfloat16), 'tp')  15.7 us
    all_to_all x1, blocking collectives, on_device(): lax.all_to_all(send_rows, 'ep', split_axis=0, concat_axis=0, tiled=True)  10.6 us
    dot_general x1, matrix products, on_device(): jnp.einsum('shpn,sn->shp', new_state, read_vec, precision=lax.Precision.H...  9.81 us
  transfers between devices with their start and end apart: 4, of which 3 were waited for; matrix products, arithmetic and copies ran while one was open for 3% of the time, Pallas kernels for 0%

profile of v1, /device:TPU:0, one launch (start us, length us, event | category | flops | bytes accessed | tf_op | source)
XLA Modules:
  0.0 214.1 jit_solution(4638022242160596109)
XLA Ops:
  7.3 1.1 fusion.31
  8.4 0.9 fusion.33
  9.4 2.0 fusion.21
  11.3 0.1 reshape.93
  11.4 0.1 convolution_convert_fusion.6
  11.6 15.7 %all-gather = bf16[128,512]{1,0:T(8,128)(2,1)S(1)} all-gather(bf16[16,512]{1,0:T(8,128)(2,1)S(1)} %convolution_convert_fusion.6), channel_id=2, replica_groups=mesh['ep'=4,'tp'=8] {'tp'}, dimensions={0}, use_global_device_ids=true | all-gather | bytes 147456 | tf_op jit(solution)/shard_map/all_gather | solution.py:78
  27.3 0.1 subtract_exponential_fusion
  27.6 2.0 fusion.22
  29.8 0.1 convolution_convert_fusion.5
  29.9 29.0 %psum.14 = bf16[16,512]{1,0:T(8,128)(2,1)S(1)} all-reduce(bf16[16,512]{1,0:T(8,128)(2,1)S(1)} %convolution_convert_fusion.5), channel_id=1, replica_groups=mesh['ep'=4,'tp'=8] {'tp'}, use_global_device_ids=true, to_apply=%region_3.0 | all-reduce | flops 8192 | bytes 32768 | tf_op jit(solution)/shard_map/psum | solution.py:79
  59.2 3.1 %multiply_add_fusion = f32[16,8,64,128]{3,2,1,0:T(8,128)S(1)} fusion(f32[16,8,64,128]{3,2,1,0:T(8,128)} %param.39, f32[16,128]{1,0:T(8,128)S(1)} %convert_multiply_fusion.5, f32[16,8,64]{2,1,0:T(8,128)S(1)} %broadcast_multiply_fusion, f32[16,8]{1,0:T(8,128)S(1)} %copy.58), kind=kLoop, calls=%fused_computation | loop fusion | flops 3145728 | bytes 8430080 | tf_op jit(solution)/shard_map/add | solution.py:100
  62.3 9.8 %fusion.68 = f32[16,1,8,64]{3,1,2,0:T(1,128)S(1)} fusion(f32[16,8,64,128]{3,2,1,0:T(8,128)S(1)} %multiply_add_fusion, f32[16,128,1,1]{1,2,3,0:T(1,128)S(1)} %bitcast.74), kind=kOutput, calls=%fused_computation.95 | convolution fusion | flops 12582912 | bytes 4235264 | tf_op jit(solution)/shard_map/shpn,sn->shp/dot_general | solution.py:103
  72.2 0.2 multiply_reduce_fusion.1
  72.5 0.1 reshape.89
  72.6 2.6 %convolution_convert_fusion.3 = bf16[16,2048]{1,0:T(8,128)(2,1)} fusion(bf16[16,512]{1,0:T(8,128)(2,1)S(1)} %reshape.89, bf16[512,2048]{1,0:T(8,128)(2,1)} %param.42), kind=kOutput, calls=%fused_computation.5 | convolution fusion | flops 33587200 | bytes 2179072 | tf_op jit(solution)/shard_map/dot_general | solution.py:108
  75.5 0.1 reduce_window_sum.11
  75.6 0.2 select_reduce_fusion.1
  75.9 0.1 copy.61
  76.0 52.3 %all-reduce.2.cloned.1.call-done = bf16[16,2048]{1,0:T(8,128)(2,1)} async-done(((bf16[16,2048]{1,0:T(8,128)(2,1)}), bf16[16,2048]{1,0:T(8,128)(2,1)}) %all-reduce.2.cloned.1.call-update) | async-done | bytes 65552 | tf_op jit(solution)/shard_map/psum | solution.py:109
  128.4 1.0 fusion.28
  129.4 0.3 convolution_convert_fusion.1
  129.7 10.6 %all_to_all.10 = bf16[4,2,16,2048]{3,2,1,0:T(8,128)(2,1)S(1)} all-to-all(bf16[4,2,16,2048]{3,2,1,0:T(8,128)(2,1)S(1)} %bitcast.70), channel_id=1, replica_groups=mesh['ep'=4,'tp'=8] {'ep'}, dimensions={0} | all-to-all | bytes 1048576 | tf_op jit(solution)/shard_map/all_to_all | solution.py:132
  140.3 2.0 fusion.7
  142.3 3.3 %fusion = bf16[4,2,16,2048]{3,2,0,1:T(8,128)(2,1)} fusion(bf16[2,256,2048]{2,1,0:T(8,128)(2,1)S(1)} %copy-done, bf16[2,2048,256]{2,1,0:T(8,128)(2,1)} %param.45, bf16[4,2,16,2048]{3,2,1,0:T(8,128)(2,1)S(1)} %all_to_all.10, f32[4,2,16,256]{3,2,0,1:T(8,128)S(1)} %fusion.7), kind=kOutput, calls=%fused_computation.3 | convolution fusion | flops 268894208 | bytes 5373952 | tf_op jit(solution)/shard_map/ajcf,jfd->ajcd/dot_general | solution.py:35
  145.7 1.5 fusion.65
  147.2 2.9 %fusion.1 = bf16[1,1,16,2048]{3,2,1,0:T(8,128)(2,1)} fusion(bf16[256,2048]{1,0:T(8,128)(2,1)} %param.49, bf16[2048,256]{1,0:T(8,128)(2,1)} %param.48, f32[16,256]{1,0:T(8,128)S(1)} %fusion.65, bf16[16,2048]{1,0:T(8,128)(2,1)S(1)} %get-tuple-element.4, f32[2048]{0:T(1024)S(1)} %copy-done.6, f32[16]{0:T(128)S(1)} %add_rsqrt_fusion.1), kind=kOutput, calls=%fused_computation.6 | convolution fusion | flops 33742848 | bytes 2252864 | tf_op jit(solution)/shard_map/dot_general | solution.py:117
  150.3 25.1 %reduce-scatter.5.cloned.1.call-done = bf16[4,2,16,256]{3,2,0,1:T(8,128)(2,1)} async-done(((bf16[4,2,16,2048]{3,2,0,1:T(8,128)(2,1)}), bf16[4,2,16,256]{3,2,0,1:T(8,128)(2,1)}) %reduce-scatter.5.cloned.1.call-update) | async-done | bytes 65552 | tf_op jit(solution)/shard_map/reduce_scatter | solution.py:138
  175.4 1.5 copy.64
  176.9 3.5 %all-to-all-start.1 = ((bf16[4,2,16,256]{3,2,1,0:T(8,128)(2,1)}), bf16[4,2,16,256]{3,2,1,0:T(8,128)(2,1)S(1)}, u32[]{:S(2)}, u32[]{:S(2)}) async-start(bf16[4,2,16,256]{3,2,1,0:T(8,128)(2,1)} %copy.64), calls=%async_computation.3 | async-start | bytes 131072 | tf_op jit(solution)/shard_map/all_to_all | solution.py:149
  180.4 0.6 fusion.41
  181.0 25.2 %reduce-scatter.3.cloned.1.call-done = bf16[1,1,16,256]{3,2,1,0:T(8,128)(2,1)} async-done(((bf16[1,1,16,2048]{3,2,1,0:T(8,128)(2,1)}), bf16[1,1,16,256]{3,2,1,0:T(8,128)(2,1)}) %reduce-scatter.3.cloned.1.call-update) | async-done | bytes 8208 | tf_op jit(solution)/shard_map/reduce_scatter | solution.py:141
  206.2 1.4 fusion.24
  (61 shorter events, 1.3 us)
Async XLA Ops:
  7.2 135.2 %copy-start = (bf16[2,256,2048]{2,1,0:T(8,128)(2,1)S(1)}, bf16[2,256,2048]{2,1,0:T(8,128)(2,1)}, u32[]{:S(2)}) copy-start(bf16[2,256,2048]{2,1,0:T(8,128)(2,1)} %param.46) | copy-start | bytes 6291460
  7.2 4.3 %copy-start.3 = (bf16[256,512]{1,0:T(8,128)(2,1)S(1)}, bf16[256,512]{1,0:T(8,128)(2,1)}, u32[]{:S(2)}) copy-start(bf16[256,512]{1,0:T(8,128)(2,1)} %param.32) | copy-start | bytes 786436
  7.2 20.1 %copy-start.14 = (f32[8]{0:T(128)S(1)}, f32[8]{0:T(128)}, u32[]{:S(2)}) copy-start(f32[8]{0:T(128)} %param.35) | copy-start | bytes 100
  7.2 20.1 %copy-start.13 = (f32[16,8]{0,1:T(8,128)S(1)}, f32[16,8]{0,1:T(8,128)}, u32[]{:S(2)}) copy-start(f32[16,8]{0,1:T(8,128)} %param.36) | copy-start | bytes 1540
  7.2 20.1 %copy-start.15 = (f32[8]{0:T(128)S(1)}, f32[8]{0:T(128)}, u32[]{:S(2)}) copy-start(f32[8]{0:T(128)} %param.34) | copy-start | bytes 100
  7.2 20.1 %copy-start.12 = (bf16[2048,8]{0,1:T(8,128)(2,1)S(1)}, bf16[2048,8]{0,1:T(8,128)(2,1)}, u32[]{:S(2)}) copy-start(bf16[2048,8]{0,1:T(8,128)(2,1)} %param.31) | copy-start | bytes 98308
  7.2 121.1 %all-reduce.2.cloned.1.call-start = ((), (), s32[]{:S(2)}) async-start(), calls=%async_computation.4 | async-start | bytes 131072 | tf_op jit(solution)/shard_map/psum | solution.py:109
  9.3 20.2 %copy-start.8 = (bf16[4,512]{1,0:T(4,128)(2,1)S(1)}, bf16[4,512]{1,0:T(4,128)(2,1)}, u32[]{:S(2)}) copy-start(bf16[4,512]{1,0:T(4,128)(2,1)} %param.37) | copy-start | bytes 12292
  9.4 20.2 %copy-start.5 = (bf16[16,3,512]{2,0,1:T(8,128)(2,1)S(1)}, bf16[16,3,512]{2,0,1:T(8,128)(2,1)}, u32[]{:S(2)}) copy-start(bf16[16,3,512]{2,0,1:T(8,128)(2,1)} %param.38) | copy-start | bytes 147460
  11.3 18.4 %copy-start.4 = (bf16[256,512]{1,0:T(8,128)(2,1)S(1)}, bf16[256,512]{1,0:T(8,128)(2,1)}, u32[]{:S(2)}) copy-start(bf16[256,512]{1,0:T(8,128)(2,1)} %param.33) | copy-start | bytes 786436
  11.3 47.7 %copy-start.9 = (f32[512]{0:T(512)S(1)}, f32[512]{0:T(512)}, u32[]{:S(2)}) copy-start(f32[512]{0:T(512)} %param.41) | copy-start | bytes 6148
  62.3 9.8 %copy-start.1 = (f32[16,8,64,128]{3,2,1,0:T(8,128)}, f32[16,8,64,128]{3,2,1,0:T(8,128)S(1)}, u32[]{:S(2)}) copy-start(f32[16,8,64,128]{3,2,1,0:T(8,128)S(1)} %multiply_add_fusion) | copy-start | bytes 12582916
  62.3 9.9 %copy-start.11 = (f32[8]{0:T(128)S(1)}, f32[8]{0:T(128)}, u32[]{:S(2)}) copy-start(f32[8]{0:T(128)} %param.40) | copy-start | bytes 100
  72.1 3.1 %copy-start.7 = (s32[16,4]{0,1:T(4,128)S(1)}, s32[16,4]{0,1:T(4,128)}, u32[]{:S(2)}) copy-start(s32[16,4]{0,1:T(4,128)} %param.26) | copy-start | bytes 772
  72.1 56.2 %copy-start.2 = (bf16[16,2048]{1,0:T(8,128)(2,1)S(1)}, bf16[16,2048]{1,0:T(8,128)(2,1)}, u32[]{:S(2)}) copy-start(bf16[16,2048]{1,0:T(8,128)(2,1)} %param.25) | copy-start | bytes 196612
  72.2 57.2 %copy-start.6 = (f32[2048]{0:T(1024)S(1)}, f32[2048]{0:T(1024)}, u32[]{:S(2)}) copy-start(f32[2048]{0:T(1024)} %param.43) | copy-start | bytes 24580
  75.2 100.2 %reduce-scatter.5.cloned.1.call-start = ((), (), s32[]{:S(2)}) async-start(), calls=%async_computation.6 | async-start | bytes 589824 | tf_op jit(solution)/shard_map/reduce_scatter | solution.py:138
  145.6 4.6 %copy-start.10 = (f32[16,4]{0,1:T(4,128)S(1)}, f32[16,4]{0,1:T(4,128)}, u32[]{:S(2)}) copy-start(f32[16,4]{0,1:T(4,128)} %param.27) | copy-start | bytes 772
  145.7 60.5 %reduce-scatter.3.cloned.1.call-start = ((), (), s32[]{:S(2)}) async-start(), calls=%async_computation.5 | async-start | bytes 73728 | tf_op jit(solution)/shard_map/reduce_scatter | solution.py:141
  176.9 29.3 %all-to-all-start.1 = ((bf16[4,2,16,256]{3,2,1,0:T(8,128)(2,1)}), bf16[4,2,16,256]{3,2,1,0:T(8,128)(2,1)S(1)}, u32[]{:S(2)}, u32[]{:S(2)}) async-start(bf16[4,2,16,256]{3,2,1,0:T(8,128)(2,1)} %copy.64), calls=%async_computation.3 | async-start | bytes 131072 | tf_op jit(solution)/shard_map/all_to_all | solution.py:149
Sparse Core Ops, SparseCore 0:
  75.3 53.0 all-reduce.1
  145.8 29.5 reduce-scatter.4
  177.6 28.4 reduce-scatter.2
